TPU v7x, 32 devices: a whole 2x2x4 slice. The times are simulated.
32 devices in a mesh: sp: 8 (over z, y), tp: 4 (over x, core).
Axes of the slice: x: 2, y: 2, z: 4, core: 2. Of those that a mesh axis runs over, the one named last changes fastest.
Arguments:
- stream: bfloat16 [2048, 2048], P('sp'), may hold values from -3 to 3
- first_group_queries: bfloat16 [2048, 512], P('sp', 'tp'), may hold values from -6 to 6
- first_group_keys: bfloat16 [2048, 512], P('sp', 'tp'), may hold values from -6 to 6
- first_group_values: bfloat16 [2048, 1024], P('sp', 'tp'), may hold values from -5.5 to 5.5
- first_gate_logits: bfloat16 [2048, 1024], P('sp', 'tp'), may hold values from -6 to 6
- first_decay_logits: bfloat16 [2048, 512], P('sp', 'tp'), may hold values from -4.75 to 14.5
- second_group_queries: bfloat16 [2048, 1024], P('sp', 'tp'), may hold values from -6 to 6
- second_group_keys: bfloat16 [2048, 1024], P('sp', 'tp'), may hold values from -6 to 6
- second_group_values: bfloat16 [2048, 1024], P('sp', 'tp'), may hold values from -5.5 to 5.5
- second_gate_logits: bfloat16 [2048, 1024], P('sp', 'tp'), may hold values from -6 to 6
- second_decay_logits: bfloat16 [2048, 1024], P('sp', 'tp'), may hold values from -4.75 to 14.5
- position_log_decay: float32 [2048], P('sp'), may hold values from -0.6932 to 0, as said below
- per_head_norm_gain: float32 [128], replicated, may hold values from 0.1 to 1.9
- first_output_weight: bfloat16 [1024, 2048], P('tp'), may hold values from -0.125 to 0.125
- second_output_weight: bfloat16 [1024, 2048], P('tp'), may hold values from -0.125 to 0.125
- feedforward_norm_gain: float32 [2048], replicated, may hold values from 0.1 to 1.9
- gate_weight: bfloat16 [2048, 5632], P('sp', 'tp'), may hold values from -0.125 to 0.125
- up_weight: bfloat16 [2048, 5632], P('sp', 'tp'), may hold values from -0.125 to 0.125
- down_weight: bfloat16 [5632, 2048], P('tp', 'sp'), may hold values from -0.078125 to 0.078125
Outputs:
- refined: bfloat16 [2048, 2048], P(('sp', 'tp'))
Inputs may be any that keep to these rules, and one draw needn't show every extreme that they name: `position_log_decay`: most positions carry 0.
All inputs are finite; a program needn't handle non-finite values.
Results may differ from a plain program's by a relative error of at most 0.018.
Values may be sent and summed in bfloat16 or wider, within the bound.
A program may use at most 64 MiB of HBM per device.

v0:
```python
import functools

import jax
import jax.numpy as jnp
from jax import lax
from jax.experimental import pallas as pl
from jax.experimental.pallas import tpu as pltpu
from jax.sharding import PartitionSpec as P

KEY_SIZE_FIRST = 64
KEY_SIZE_SECOND = 128
DV = 128
BLK = 64

decay_softness = 16.0
norm_eps = 1e-06

f32 = jnp.float32
bf16 = jnp.bfloat16
NT = (((1,), (1,)), ((), ()))
TN = (((0,), (0,)), ((), ()))


def dot(a, b, dims=None):
    if dims is None:
        return jnp.dot(a, b, preferred_element_type=f32)
    return lax.dot_general(a, b, dims, preferred_element_type=f32)


def log_decay_sums(decay_ref, pos_ref):
    x = decay_ref[...].astype(f32)
    log_decay = -jax.nn.softplus(-x) / decay_softness + pos_ref[...]
    length = x.shape[0]
    at = lax.broadcasted_iota(jnp.int32, (length, length), 0)
    of = lax.broadcasted_iota(jnp.int32, (length, length), 1)
    tri = jnp.where(at >= of, 1.0, 0.0).astype(f32)
    upto = jnp.dot(tri, log_decay, preferred_element_type=f32, precision=lax.Precision.HIGHEST)
    return upto, upto - log_decay


def lane_mask(width, key_channels, head):
    lanes = lax.broadcasted_iota(jnp.int32, (1, width), 1)
    return (lanes >= head * key_channels) & (lanes < (head + 1) * key_channels)


def head_groups(width, key_channels):
    span = min(width, 128)
    return [(s, span, span // key_channels) for s in range(0, width, span)]


def states_kernel(ka, va, da, kb, vb, db, pos, fwd, bwd, tot):
    at = 0
    for k_ref, v_ref, d_ref, size in ((kb, vb, db, KEY_SIZE_SECOND), (ka, va, da, KEY_SIZE_FIRST)):
        upto, before = log_decay_sums(d_ref, pos)
        last = upto[-1:, :]
        k = k_ref[...].astype(f32)
        ahead = (k * jnp.exp(last - upto)).astype(bf16)
        behind = (k * jnp.exp(before)).astype(bf16)
        head = 0
        for start, span, heads in head_groups(k.shape[1], size):
            f = b = None
            for h in range(heads):
                v = v_ref[:, head * DV : (head + 1) * DV]
                fh = dot(v, ahead[:, start : start + span], TN)
                bh = dot(v, behind[:, start : start + span], TN)
                if f is None:
                    f, b = fh, bh
                else:
                    m = lane_mask(span, size, h)
                    f, b = jnp.where(m, fh, f), jnp.where(m, bh, b)
                head += 1
            fwd[:, at : at + span] = f
            bwd[:, at : at + span] = b
            tot[:, at : at + span] = jnp.broadcast_to(last[:, start : start + span], (16, span))
            at += span


def attend_kernel(
    qa, ka, va, ga, da, qb, kb, vb, gb, db, pos, gain, wa, wb, fwd, bwd, out, mixed
):
    at = 0
    base = 0
    length = qa.shape[0]
    row = lax.broadcasted_iota(jnp.int32, (BLK, length), 0)
    col = lax.broadcasted_iota(jnp.int32, (BLK, length), 1)
    for q_ref, k_ref, v_ref, g_ref, d_ref, size in (
        (qb, kb, vb, gb, db, KEY_SIZE_SECOND),
        (qa, ka, va, ga, da, KEY_SIZE_FIRST),
    ):
        upto_all, before_all = log_decay_sums(d_ref, pos)
        head = 0
        for start, span, heads in head_groups(q_ref.shape[1], size):
            cut = slice(start, start + span)
            upto, before = upto_all[:, cut], before_all[:, cut]
            q = q_ref[:, cut].astype(f32)
            k = k_ref[:, cut].astype(f32)
            total = upto[-1:, :]
            fs = fwd[:, at : at + span].astype(bf16)
            bs = bwd[:, at : at + span].astype(bf16)
            at += span
            for block in range(length // BLK):
                lo, hi = block * BLK, (block + 1) * BLK
                start_log = before[lo : lo + 1, :]
                end_log = upto[hi - 1 : hi, :]
                qi = q[lo:hi]
                q_f = qi * jnp.exp(upto[lo:hi] - start_log)
                q_b = qi * jnp.exp(end_log - before[lo:hi])
                k_f = (k[:hi] * jnp.exp(start_log - upto[:hi])).astype(bf16)
                k_b = (k[lo:] * jnp.exp(before[lo:] - end_log)).astype(bf16)
                q_fs = qi * jnp.exp(upto[lo:hi])
                q_bs = qi * jnp.exp(total - before[lo:hi])
                for h in range(heads):
                    if heads > 1:
                        m = lane_mask(span, size, h)
                        qf, qb_, qfs, qbs = (
                            jnp.where(m, x, 0.0).astype(bf16) for x in (q_f, q_b, q_fs, q_bs)
                        )
                    else:
                        qf, qb_, qfs, qbs = (x.astype(bf16) for x in (q_f, q_b, q_fs, q_bs))
                    vc = slice((head + h) * DV, (head + h + 1) * DV)
                    s_f = jnp.where(
                        row[:, :hi] + lo >= col[:, :hi], dot(qf, k_f, NT), 0.0
                    ).astype(bf16)
                    s_b = jnp.where(
                        row[:, : length - lo] <= col[:, : length - lo], dot(qb_, k_b, NT), 0.0
                    ).astype(bf16)
                    both = dot(s_f, v_ref[:hi, vc]) + dot(s_b, v_ref[lo:, vc])
                    both = both + dot(qfs, fs, NT) + dot(qbs, bs, NT)
                    scale = lax.rsqrt(jnp.mean(both * both, axis=-1, keepdims=True) + norm_eps)
                    g = g_ref[lo:hi, vc].astype(f32)
                    silu = g / (1.0 + jnp.exp(-g))
                    oc = slice(base + (head + h) * DV, base + (head + h + 1) * DV)
                    mixed[lo:hi, oc] = (both * scale * gain[...] * silu).astype(bf16)
            head += heads
        base += head * DV
    nb = wb.shape[0]
    width = wb.shape[1]
    step = 512
    for c in range(0, width, step):
        part = dot(mixed[:, :nb], wb[:, c : c + step]) + dot(mixed[:, nb:], wa[:, c : c + step])
        out[:, :, :, c : c + step] = part.astype(bf16).reshape(out.shape[:3] + (step,))


def flip_bit(index, bit):
    return index + bit - 2 * bit * (index // bit % 2)


def shifted(index, mask):
    bit = 1
    while bit <= mask:
        if mask & bit:
            index = flip_bit(index, bit)
        bit *= 2
    return index


def layer_kernel(
    n,
    tp,
    stream,
    qa, ka, va, ga, da,
    qb, kb, vb, gb, db,
    pos,
    gain,
    wa, wb,
    norm_gain,
    mine_g, mine_u, mine_d,
    far_g, far_u, far_d,
    out,
    weights_g, weights_u, weights_d,
    grp_f, grp_b, pre_f, pre_b, tot,
    scan_out, scan_in,
    mixed, partial, residual, rows_all, gate_acc, down_part,
    *rest,
):
    levels = tp.bit_length() - 1
    rest = list(rest)
    recv1 = [rest.pop(0) for _ in range(levels)]
    send1 = [rest.pop(0) for _ in range(levels - 1)]
    recv2 = [rest.pop(0) for _ in range(levels)]
    send2 = [rest.pop(0) for _ in range(levels - 1)]
    acc = [rest.pop(0) for _ in range(levels - 1)]
    last_out, last_in, hidden, w_sem, scan_sem, tp_sem, row_sem, last_sem, own_sem = rest
    me = lax.axis_index("sp")
    my_tp = lax.axis_index("tp")
    half = n // 2
    sp_bits = [1 << j for j in range(n.bit_length() - 1)]
    tp_bits = [1 << j for j in range(levels)]
    rows = residual.shape[0]

    barrier = pltpu.get_barrier_semaphore()
    for bit in sp_bits:
        pl.semaphore_signal(
            barrier, inc=1, device_id={"sp": flip_bit(me, bit)}, device_id_type=pl.DeviceIdType.MESH
        )
    for bit in tp_bits:
        pl.semaphore_signal(
            barrier,
            inc=1,
            device_id={"tp": flip_bit(my_tp, bit)},
            device_id_type=pl.DeviceIdType.MESH,
        )
    pl.semaphore_wait(barrier, len(sp_bits) + len(tp_bits))

    def remote(src, dst, sems, axis, bit):
        place = me if axis == "sp" else my_tp
        return pltpu.make_async_remote_copy(
            src_ref=src,
            dst_ref=dst,
            send_sem=sems[0],
            recv_sem=sems[1],
            device_id={axis: flip_bit(place, bit)},
            device_id_type=pl.DeviceIdType.MESH,
        )

    low = [b for b in sp_bits if b < half]
    weights = (
        (weights_g, mine_g, far_g, low),
        (weights_u, mine_u, far_u, low[::-1]),
        (weights_d, mine_d, far_d, low[::-1]),
    )
    copies = {}

    def send(w, at, bit):
        store, mine, far, _ = weights[w]
        if bit == half:
            src = far
        elif at == 0:
            src = mine
        else:
            src = store.at[shifted(me, at)]
        place = me if at == 0 else shifted(me, at)
        sems = (w_sem.at[0, w, at | bit], w_sem.at[1, w, at | bit])
        copies[w, at | bit] = remote(src, store.at[place], sems, "sp", bit)
        copies[w, at | bit].start()

    sent = set()

    def offer(w, at, bit):
        if (w, at, bit) not in sent:
            sent.add((w, at, bit))
            send(w, at, bit)

    def onward(w, at):
        order = weights[w][3]
        low_part = at & (half - 1)
        used = [order.index(b) for b in order if low_part & b]
        return order[max(used) + 1 if used else 0 :]

    own = [
        pltpu.make_async_copy(mine, store.at[me], own_sem.at[i])
        for i, (store, mine, _, _) in enumerate(weights)
    ]
    for copy in own:
        copy.start()
    for w in (0, 1):
        offer(w, 0, half)
        offer(w, 0, low[0])

    states_kernel(ka, va, da, kb, vb, db, pos, grp_f, grp_b, tot)
    pre_f[...] = jnp.zeros_like(pre_f)
    pre_b[...] = jnp.zeros_like(pre_b)
    before = jnp.zeros((1, tot.shape[1]), f32)
    after = before
    group = tot[0:1]
    for step, bit in enumerate(sp_bits):
        high = group.astype(bf16)
        rest_of = (group - high.astype(f32)).astype(bf16)
        scan_out[step, :DV] = grp_f[...].astype(bf16)
        scan_out[step, DV : 2 * DV] = grp_b[...].astype(bf16)
        scan_out[step, 2 * DV : 2 * DV + 16] = jnp.broadcast_to(high.astype(f32), tot.shape).astype(bf16)
        scan_out[step, 2 * DV + 16 :] = jnp.broadcast_to(rest_of.astype(f32), tot.shape).astype(bf16)
        copy = remote(
            scan_out.at[step],
            scan_in.at[step],
            (scan_sem.at[0, step], scan_sem.at[1, step]),
            "sp",
            bit,
        )
        copy.start()
        copy.wait()
        got_f = scan_in[step, :DV].astype(f32)
        got_b = scan_in[step, DV : 2 * DV].astype(f32)
        got_t = (
            scan_in[step, 2 * DV : 2 * DV + 16].astype(f32)
            + scan_in[step, 2 * DV + 16 :].astype(f32)
        )[0:1]
        up = jnp.full((1, tot.shape[1]), me // bit % 2, jnp.int32).astype(f32)
        down = 1.0 - up
        pre_f[...] += got_f * (up * jnp.exp(before))
        pre_b[...] += got_b * (down * jnp.exp(after))
        before, after = before + up * got_t, after + down * got_t
        grp_f[...] = grp_f[...] * jnp.exp(down * got_t) + got_f * jnp.exp(up * group)
        grp_b[...] = grp_b[...] * jnp.exp(up * got_t) + got_b * jnp.exp(down * group)
        group = group + got_t
        if step == 0:
            offer(0, 0, low[-1])
        if step == 1:
            offer(2, 0, half)
    for w in range(3):
        offer(w, 0, half)
        for bit in low:
            offer(w, 0, bit) if bit in onward(w, 0) else None

    attend_kernel(
        qa, ka, va, ga, da, qb, kb, vb, gb, db, pos, gain, wa, wb, pre_f, pre_b, partial, mixed
    )

    arrived = set()

    def take(w, at):
        if at == 0 or (w, at) in arrived:
            return
        arrived.add((w, at))
        copies[w, at].wait_recv()
        for bit in onward(w, at):
            offer(w, at, bit)

    def tp_sum(part, recvs, sends, number):
        value = None
        for j, bit in enumerate(tp_bits):
            odd = my_tp // bit % 2
            src = part if j == 0 else sends[j - 1]
            copy = remote(
                src.at[:, 1 - odd],
                recvs[j],
                (tp_sem.at[0, number, j], tp_sem.at[1, number, j]),
                "tp",
                bit,
            )
            copy.start()
            yield
            copy.wait()
            size = recvs[j].shape[1]
            if j == 0:
                kept = part[:, pl.ds(odd, 1)]
            else:
                kept = acc[j - 1][:, pl.ds(odd, 1), :size]
            value = kept[:, 0].astype(f32) + recvs[j][...].astype(f32)
            if j < levels - 1:
                shape = (value.shape[0] // 2, 2) + value.shape[1:]
                acc[j][:, :, :size] = value.reshape(shape)
                sends[j][...] = value.astype(bf16).reshape(shape)
        yield value[0]

    def run(gen, between):
        value = None
        for j, value in enumerate(gen):
            if value is None and j < len(between):
                for w, at in between[j]:
                    take(w, at)
        return value

    summed = run(tp_sum(partial, recv1, send1, 0), [[(0, half), (1, half)], [(0, low[0])]])
    own_rows = pl.ds(pl.multiple_of(my_tp * rows, rows), rows)
    res = stream[own_rows, :].astype(f32) + summed
    residual[...] = res
    scale = lax.rsqrt(jnp.mean(res * res, axis=-1, keepdims=True) + norm_eps)
    rows_all[0, my_tp] = (res * scale * norm_gain[...]).astype(bf16)

    row_copies = {}

    def pass_rows(part, at, bit):
        place = shifted(my_tp, at) if at else my_tp
        ref = rows_all.at[part, place]
        number = part * tp + (at | bit)
        row_copies[part, at | bit] = remote(
            ref, ref, (row_sem.at[0, number], row_sem.at[1, number]), "tp", bit
        )
        row_copies[part, at | bit].start()

    across = remote(
        rows_all.at[0, my_tp],
        rows_all.at[1, my_tp],
        (row_sem.at[0, tp * 2], row_sem.at[1, tp * 2]),
        "sp",
        half,
    )
    across.start()
    for bit in tp_bits[::-1]:
        pass_rows(0, 0, bit)
    for w, at in ((0, low[0]), (1, half), (1, low[0]), (2, half)):
        take(w, at)
    across.wait_recv()
    for bit in tp_bits[::-1]:
        pass_rows(1, 0, bit)
    for bit in tp_bits[-2::-1]:
        for part in (0, 1):
            for at in [a for a in range(1, tp) if a % (2 * bit) == 0]:
                if not row_copies.get(("got", part, at)):
                    row_copies["got", part, at] = True
                    row_copies[part, at].wait_recv()
                pass_rows(part, at, bit)

    def by_arrival(w):
        order = weights[w][3]
        return sorted(range(1, n), key=lambda i: ((i & (half - 1)).bit_count(), i < half, i))

    first = [i for i in by_arrival(0) if (i & (half - 1)).bit_count() <= 1]
    for i in first:
        for w in range(3):
            take(w, i)
    for part in (0, 1):
        for at in range(1, tp):
            if not row_copies.get(("got", part, at)):
                row_copies["got", part, at] = True
                row_copies[part, at].wait_recv()
    for copy in own:
        copy.wait()

    span = weights_g.shape[1]
    flat = tp * rows

    def project(w, store, part):
        x = rows_all[part].reshape(flat, n * span)
        total = None
        for j in range(n):
            term = dot(x[:, j * span : (j + 1) * span], store[j])
            total = term if total is None else total + term
        return total

    for i in by_arrival(0):
        take(0, i)
    for part in (0, 1):
        gate_acc[part] = project(0, weights_g, part)
    for i in by_arrival(1):
        take(1, i)
    for part in (0, 1):
        g = gate_acc[part]
        u = project(1, weights_u, part)
        hidden[part] = (g / (1.0 + jnp.exp(-g)) * u).astype(bf16)
    for i in by_arrival(2):
        take(2, i)
    for part in (0, 1):
        for j in range(n):
            value = dot(hidden[part], weights_d[j]).astype(bf16)
            down_part[:, :, part * rows : (part + 1) * rows, j * span : (j + 1) * span] = (
                value.reshape(tp // 2, 2, rows, span)
            )
    value = run(tp_sum(down_part, recv2, send2, 1), [])
    last_out[...] = value[rows:].astype(bf16)
    residual[...] += 0.5 * value[:rows]
    copy = remote(last_out, last_in, (last_sem.at[0], last_sem.at[1]), "sp", half)
    copy.start()
    copy.wait()
    out[...] = (residual[...] + 0.5 * last_in[...].astype(f32)).astype(bf16)
    for copy in copies.values():
        copy.wait_send()
    for key, copy in row_copies.items():
        if key[0] != "got":
            copy.wait_send()
    across.wait_send()


def per_device(
    stream,
    first_group_queries,
    first_group_keys,
    first_group_values,
    first_gate_logits,
    first_decay_logits,
    second_group_queries,
    second_group_keys,
    second_group_values,
    second_gate_logits,
    second_decay_logits,
    position_log_decay,
    per_head_norm_gain,
    first_output_weight,
    second_output_weight,
    feedforward_norm_gain,
    gate_weight,
    up_weight,
    down_weight,
):
    n = lax.axis_size("sp")
    tp = lax.axis_size("tp")
    tokens, width = stream.shape
    upper = lax.axis_index("sp") >= n // 2
    units = gate_weight.shape[1] // 2
    rows = tokens // tp
    span = width // n

    def halves(first, second):
        return jnp.where(upper, second, first), jnp.where(upper, first, second)

    mine_g, far_g = halves(gate_weight[:, :units], gate_weight[:, units:])
    mine_u, far_u = halves(up_weight[:, :units], up_weight[:, units:])
    mine_d, far_d = halves(down_weight[:units], down_weight[units:])
    args = (
        stream,
        first_group_queries,
        first_group_keys,
        first_group_values,
        first_gate_logits,
        first_decay_logits,
        second_group_queries,
        second_group_keys,
        second_group_values,
        second_gate_logits,
        second_decay_logits,
        position_log_decay[:, None],
        per_head_norm_gain[None, :],
        first_output_weight,
        second_output_weight,
        feedforward_norm_gain[None, :],
        mine_g,
        mine_u,
        mine_d,
        far_g,
        far_u,
        far_d,
    )
    states = second_group_keys.shape[1] + first_group_keys.shape[1]
    heads_width = second_output_weight.shape[0] + first_output_weight.shape[0]
    levels = tp.bit_length() - 1
    steps = n.bit_length() - 1
    vm = pltpu.VMEM

    def tp_buffers(size):
        recv = [vm((tp >> (j + 1), size, width), bf16) for j in range(levels)]
        give = [vm((tp >> (j + 2), 2, size, width), bf16) for j in range(levels - 1)]
        return recv + give

    scratch = [
        vm((n, span, units), bf16),
        vm((n, span, units), bf16),
        vm((n, units, span), bf16),
        *([vm((DV, states), f32)] * 4),
        vm((16, states), f32),
        vm((steps, 2 * DV + 32, states), bf16),
        vm((steps, 2 * DV + 32, states), bf16),
        vm((tokens, heads_width), bf16),
        vm((tp // 2, 2, rows, width), bf16),
        vm((rows, width), f32),
        vm((2, tp, rows, width), bf16),
        vm((2, tokens, units), f32),
        vm((tp // 2, 2, 2 * rows, width), bf16),
        *tp_buffers(rows),
        *tp_buffers(2 * rows),
        *[vm((tp >> (j + 2), 2, 2 * rows, width), f32) for j in range(levels - 1)],
        vm((rows, width), bf16),
        vm((rows, width), bf16),
        vm((2, tokens, units), bf16),
        pltpu.SemaphoreType.DMA((2, 3, n)),
        pltpu.SemaphoreType.DMA((2, steps)),
        pltpu.SemaphoreType.DMA((2, 2, levels)),
        pltpu.SemaphoreType.DMA((2, 2 * tp + 1)),
        pltpu.SemaphoreType.DMA((2,)),
        pltpu.SemaphoreType.DMA((3,)),
    ]
    spec = pl.BlockSpec(memory_space=pltpu.VMEM)
    return pl.pallas_call(
        functools.partial(layer_kernel, n, tp),
        out_shape=jax.ShapeDtypeStruct((rows, width), bf16),
        in_specs=[spec] * len(args),
        out_specs=spec,
        scratch_shapes=scratch,
        compiler_params=pltpu.CompilerParams(
            collective_id=0, has_side_effects=True, vmem_limit_bytes=60 * 1024 * 1024
        ),
    )(*args)


def solution(mesh):
    in_specs = (
        P("sp", None),
        *([P("sp", "tp")] * 10),
        P("sp"),
        P(),
        P("tp", None),
        P("tp", None),
        P(),
        P("sp", "tp"),
        P("sp", "tp"),
        P("tp", "sp"),
    )
    out_specs = P(("sp", "tp"), None)
    return jax.shard_map(
        per_device, mesh=mesh, in_specs=in_specs, out_specs=out_specs, check_vma=False
    )
```

profile of v0, /device:TPU:0, one launch (start us, length us, event | category | flops | bytes accessed | tf_op | source)
XLA Modules:
  0.0 204.3 jit_solution(2271812490967372099)
XLA Ops:
  0.0 0.0 copy-start.2
  0.0 0.7 copy-done.2
  0.7 0.8 copy.20.pos
  1.5 0.0 copy-start
  1.5 0.0 copy-start.1
  1.5 2.1 %broadcast_select_fusion.4 = (bf16[704,256]{1,0:T(8,128)(2,1)}, bf16[704,256]{1,0:T(8,128)(2,1)}) fusion(pred[]{:T(512)S(6)} %ge.3, bf16[1408,256]{1,0:T(8,128)(2,1)} %param.37), kind=kLoop, calls=%fused_computation.4 | loop fusion | flops 360448 | bytes 1441793 | tf_op jit(solution)/shard_map/jit(_where)/select_n | solution.py:485
  3.6 0.0 copy-done
  3.6 0.0 copy-done.1
  3.6 1.4 broadcast_select_fusion
  5.1 197.5 %shard_map.181 = bf16[64,2048]{1,0:T(8,128)(2,1)} custom-call(bf16[256,2048]{1,0:T(8,128)(2,1)} %stream.1, bf16[256,128]{1,0:T(8,128)(2,1)} %qa.1, bf16[256,128]{1,0:T(8,128)(2,1)} %ka.1, bf16[256,256]{1,0:T(8,128)(2,1)} %va.1, bf16[256,256]{1,0:T(8,128)(2,1)} %ga.1, bf16[256,128]{1,0:T(8,128)(2,1)} %da.1, bf16[256,256]{1,0:T(8,128)(2,1)} %qb.1, ...), custom_call_target="tpu_custom_call" | custom-call | tf_op jit(solution)/shard_map/pallas_call | solution.py:553
  202.6 1.7 copy.22
Async XLA Ops:
  0.0 0.7 copy-start.2
  1.5 2.1 %copy-start = (bf16[256,1408]{1,0:T(8,128)(2,1)S(1)}, bf16[256,1408]{1,0:T(8,128)(2,1)}, u32[]{:S(2)}) copy-start(bf16[256,1408]{1,0:T(8,128)(2,1)} %param.36) | copy-start | bytes 2162692
  1.5 2.1 %copy-start.1 = (bf16[256,1408]{1,0:T(8,128)(2,1)S(1)}, bf16[256,1408]{1,0:T(8,128)(2,1)}, u32[]{:S(2)}) copy-start(bf16[256,1408]{1,0:T(8,128)(2,1)} %param.35) | copy-start | bytes 2162692
where the time goes:
time: 204 us
  Pallas kernels  198 us (97%)
  other arithmetic  3.58 us (2%)
  local copies, waits for them, and re-layouts  3.16 us (2%)
    pallas_call x1, Pallas kernels, per_device(): pl.pallas_call(functools.partial(layer_kernel, n, tp), out_shape=jax.Shap...  198 us

commit v1 on v0

--- a/solution.py
+++ b/solution.py
@@ -253,9 +253,10 @@
     ]
     for copy in own:
         copy.start()
-    for w in (0, 1):
+    for w in (0, 1, 2):
         offer(w, 0, half)
-        offer(w, 0, low[0])
+        for bit in low:
+            offer(w, 0, bit)
 
     states_kernel(ka, va, da, kb, vb, db, pos, grp_f, grp_b, tot)
     pre_f[...] = jnp.zeros_like(pre_f)

time: 204 us -> 188 us (0.922)
  Pallas kernels: 198 us -> 181 us
    pallas_call x1, Pallas kernels: 198 us -> 181 us  [per_device(): pl.pallas_call(functools.partial(layer_kernel, n, tp), out_shape=jax.Shap...]
where the time goes in v1:
time: 188 us; the launch traced here: 187 us
  Pallas kernels  181 us (96%)
  other arithmetic  3.58 us (2%)
  local copies, waits for them, and re-layouts  3.16 us (2%)
    pallas_call x1, Pallas kernels, per_device(): pl.pallas_call(functools.partial(layer_kernel, n, tp), out_shape=jax.Shap...  181 us

profile of v1, /device:TPU:0, one launch (start us, length us, event | category | flops | bytes accessed | tf_op | source)
XLA Modules:
  0.0 187.4 jit_solution(5465740923247152949)
XLA Ops:
  0.0 0.0 copy-start.2
  0.0 0.7 copy-done.2
  0.7 0.8 copy.20.pos
  1.5 0.0 copy-start
  1.5 0.0 copy-start.1
  1.5 2.1 %broadcast_select_fusion.4 = (bf16[704,256]{1,0:T(8,128)(2,1)}, bf16[704,256]{1,0:T(8,128)(2,1)}) fusion(pred[]{:T(512)S(6)} %ge.3, bf16[1408,256]{1,0:T(8,128)(2,1)} %param.37), kind=kLoop, calls=%fused_computation.4 | loop fusion | flops 360448 | bytes 1441793 | tf_op jit(solution)/shard_map/jit(_where)/select_n | solution.py:486
  3.6 0.0 copy-done
  3.6 0.0 copy-done.1
  3.6 1.4 broadcast_select_fusion
  5.1 180.7 %shard_map.181 = bf16[64,2048]{1,0:T(8,128)(2,1)} custom-call(bf16[256,2048]{1,0:T(8,128)(2,1)} %stream.1, bf16[256,128]{1,0:T(8,128)(2,1)} %qa.1, bf16[256,128]{1,0:T(8,128)(2,1)} %ka.1, bf16[256,256]{1,0:T(8,128)(2,1)} %va.1, bf16[256,256]{1,0:T(8,128)(2,1)} %ga.1, bf16[256,128]{1,0:T(8,128)(2,1)} %da.1, bf16[256,256]{1,0:T(8,128)(2,1)} %qb.1, ...), custom_call_target="tpu_custom_call" | custom-call | tf_op jit(solution)/shard_map/pallas_call | solution.py:554
  185.8 1.7 copy.22
Async XLA Ops:
  0.0 0.7 copy-start.2
  1.5 2.1 %copy-start = (bf16[256,1408]{1,0:T(8,128)(2,1)S(1)}, bf16[256,1408]{1,0:T(8,128)(2,1)}, u32[]{:S(2)}) copy-start(bf16[256,1408]{1,0:T(8,128)(2,1)} %param.36) | copy-start | bytes 2162692
  1.5 2.1 %copy-start.1 = (bf16[256,1408]{1,0:T(8,128)(2,1)S(1)}, bf16[256,1408]{1,0:T(8,128)(2,1)}, u32[]{:S(2)}) copy-start(bf16[256,1408]{1,0:T(8,128)(2,1)} %param.35) | copy-start | bytes 2162692
